TPU v7x, 512 devices: a whole 4x4x16 slice. The times are simulated.
512 devices in a mesh: ep: 32 (over z, core), tp: 16 (over y, x).
Axes of the slice: x: 4, y: 4, z: 16, core: 2. Of those that a mesh axis runs over, the one named last changes fastest.
Arguments:
- queries: bfloat16 [8192, 2048], P('ep', 'tp'), may hold values from -6 to 6
- keys: bfloat16 [8192, 2048], P('ep', 'tp'), may hold values from -6 to 6
- values: bfloat16 [8192, 2048], P('ep', 'tp'), may hold values from -6 to 6
- gates: bfloat16 [8192, 2048], P('ep', 'tp'), may hold values from -6 to 6
- log_decay: float32 [8192, 16], P('ep', 'tp'), may hold values from -2 to 0
- out_weight: bfloat16 [2048, 2048], P(None, 'tp'), may hold values from -0.125 to 0.125
- moe_rows: bfloat16 [8192, 2048], P('ep'), may hold values from -140 to 140
- moe_gain: bfloat16 [2048], replicated, may hold values from 0.099609375 to 1.8984375
- routes: int32 [8192, 2], P('ep'), may hold values from 0 to 31, as said below
- route_weights: float32 [8192, 2], P('ep'), may hold values from 0.1 to 1
- gate_proj: bfloat16 [32, 2048, 4096], P('ep', None, 'tp'), may hold values from -0.125 to 0.125
- up_proj: bfloat16 [32, 2048, 4096], P('ep', None, 'tp'), may hold values from -0.125 to 0.125
- down_proj: bfloat16 [32, 4096, 2048], P('ep', None, 'tp'), may hold values from -0.09375 to 0.09375
Outputs:
- mixer_out: bfloat16 [8192, 2048], P('ep', 'tp')
- moe_out: bfloat16 [8192, 2048], P('ep', 'tp')
Inputs may be any that keep to these rules, and one draw needn't show every extreme that they name: `routes`: each row names two different experts of one group of 8 consecutive experts; in each aligned block of 256 rows every expert is named by exactly 16 rows.
All inputs are finite; a program needn't handle non-finite values.
Results may differ from a plain program's by a relative error of at most 0.011.
Values may be sent and summed in bfloat16 or wider, within the bound.
No kernel may reach another device: no remote copies, remote signals or barrier semaphores. Data moves between devices by JAX's collectives and lax.ppermute only.
A program may use at most 64 MiB of HBM per device.

v0:
```python
import jax
import jax.numpy as jnp
from jax import lax
from jax.sharding import Mesh
from jax.sharding import PartitionSpec as P

BLOCK = 128
EP = ("ep_0", "ep_1")
TP = ("tp_0", "tp_1")


def filled_with(array, identity):
    return jax.tree.map(
        lambda part, zero: jnp.zeros_like(part) + jnp.asarray(zero, part.dtype), array, identity
    )


def collected_together(array, axis):
    leaves = jax.tree.leaves(array)
    turns = sorted(range(len(leaves)), key=lambda k: -leaves[k].size)
    width = (1, *leaves[turns[0]].shape)[-1]
    lines = [
        jnp.pad(leaves[k].reshape(-1), (0, -leaves[k].size % width)).reshape(-1, width)
        for k in turns
    ]
    both, at, found = (lax.all_gather(jnp.concatenate(lines), axis), 0, {})
    for k, line in zip(turns, lines):
        piece = both[:, at : at + len(line)].reshape(len(both), -1)
        found[k] = piece[:, : leaves[k].size].reshape(-1, *leaves[k].shape)
        at += len(line)
    numbers = iter(range(len(leaves)))
    return jax.tree.map(lambda _: found[next(numbers)], array)


def carried_in(array, axes, combine, identity):
    before = start = filled_with(array, identity)
    total = array
    for axis in reversed(axes):
        peers, mine = (lax.axis_size(axis), lax.axis_index(axis))
        pieces = collected_together(total, axis)
        inside, total = (start, start)
        for k in range(peers):
            passed = k < mine
            total = combine(total, jax.tree.map(lambda part: part[k], pieces))
            inside = jax.tree.map(lambda new, old: jnp.where(passed, new, old), total, inside)
        before = combine(inside, before)
    return before


def whole_of(array, axes, dim):
    for axis in reversed(axes):
        array = lax.all_gather(array, axis, axis=dim, tiled=True)
    return array


def in_order(parts, dim):
    lengths = list(parts.shape[1:])
    lengths[dim] *= parts.shape[0]
    return jnp.moveaxis(parts, 0, dim).reshape(lengths)


def copy_for_each(array, axis):
    peers = lax.axis_size(axis)
    return lax.all_to_all(
        jnp.broadcast_to(array[None], (peers, *array.shape)), axis, 0, 0, tiled=True
    )


def collect(array, axis, dim):
    return in_order(copy_for_each(array, axis), dim)


def rotate(source, positions, heads_here, factor):
    row_count, feat_width = source.shape
    head_dim = feat_width // heads_here
    half_dim = head_dim // 2
    values_f = source.astype(jnp.float32).reshape(row_count, heads_here, head_dim)
    inverse = 10000.0 ** (-jnp.arange(half_dim, dtype=jnp.float32) / half_dim)
    angles = positions[:, None] * inverse[None, :]
    cosine = jnp.cos(angles)[:, None, :]
    sine_part = jnp.sin(angles)[:, None, :]
    first_half = values_f[..., :half_dim]
    second_half = values_f[..., half_dim:]
    turned = jnp.concatenate(
        [
            first_half * cosine - second_half * sine_part,
            first_half * sine_part + second_half * cosine,
        ],
        axis=-1,
    )
    return (turned * factor).astype(jnp.bfloat16).reshape(row_count, feat_width)


def chain_states(earlier, later):
    return (earlier[0] * later[0], later[0][:, None, None] * earlier[1] + later[1])


def retention_half(queries, keys, values, gates, log_decay, out_weight):
    row_count, feat_width = queries.shape
    heads_here = log_decay.shape[1]
    head_dim = feat_width // heads_here
    block_count = row_count // BLOCK
    positions = (lax.axis_index(EP) * row_count + jnp.arange(row_count, dtype=jnp.int32)).astype(
        jnp.float32
    )
    rot_q = rotate(queries, positions, heads_here, 1.0)
    rot_k = rotate(keys, positions, heads_here, head_dim ** (-0.5))
    block_shape = (block_count, BLOCK, heads_here, head_dim)
    q_blocks = rot_q.reshape(block_shape)
    k_blocks = rot_k.reshape(block_shape)
    v_blocks = values.reshape(block_shape)
    cumulative = jnp.cumsum(log_decay.reshape(block_count, BLOCK, heads_here), axis=1)
    across = jnp.swapaxes(cumulative, 1, 2)
    spread = across[..., :, None] - across[..., None, :]
    causal = jnp.arange(BLOCK)[:, None] >= jnp.arange(BLOCK)[None, :]
    weights = jnp.where(causal, jnp.exp(jnp.where(causal, spread, 0.0)), 0.0)
    scores = jnp.einsum("nihd,njhd->nhij", q_blocks, k_blocks, preferred_element_type=jnp.float32)
    rounded = (scores * weights).astype(jnp.bfloat16)
    inside = jnp.einsum("nhij,njhd->nihd", rounded, v_blocks, preferred_element_type=jnp.float32)
    ending = cumulative[:, -1, :]
    k_scaled = k_blocks.astype(jnp.float32) * jnp.exp(ending[:, None, :] - cumulative)[..., None]
    updates = jnp.einsum(
        "njhd,njhe->nhde", k_scaled, v_blocks.astype(jnp.float32), precision=lax.Precision.HIGHEST
    )

    def advance(carry_state, member):
        return (jnp.exp(member[0])[:, None, None] * carry_state + member[1], carry_state)

    zero_state = jnp.zeros((heads_here, head_dim, head_dim), jnp.float32)
    local_end, before = lax.scan(advance, zero_state, (ending, updates))
    device_decay = jnp.exp(jnp.sum(ending, axis=0))
    incoming = carried_in(
        (device_decay, local_end), EP, chain_states, (jnp.ones_like(device_decay), zero_state)
    )
    leading = jnp.cumsum(ending, axis=0) - ending
    entering = before + jnp.exp(leading)[:, :, None, None] * incoming[1][None]
    carried = (
        jnp.einsum(
            "nihd,nhde->nihe",
            q_blocks.astype(jnp.float32),
            entering,
            precision=lax.Precision.HIGHEST,
        )
        * jnp.exp(cumulative)[..., None]
    )
    retained = (inside + carried).reshape(row_count, heads_here, head_dim)
    gate_f = gates.astype(jnp.float32).reshape(row_count, heads_here, head_dim)
    scaled = retained * lax.rsqrt(jnp.mean(retained * retained, axis=-1, keepdims=True) + 1e-05)
    head_out = (scaled * jax.nn.silu(gate_f)).astype(jnp.bfloat16).reshape(row_count, feat_width)
    projected = jnp.dot(whole_of(head_out, TP, 1), out_weight, preferred_element_type=jnp.float32)
    return projected.astype(jnp.bfloat16)


def expert_half(moe_rows, moe_gain, routes, route_weights, gate_proj, up_proj, down_proj):
    row_count, feat_width = moe_rows.shape
    experts = lax.axis_size(EP)
    capacity = 2 * row_count // experts
    as_float = moe_rows.astype(jnp.float32)
    normed = (
        as_float
        * lax.rsqrt(jnp.mean(as_float * as_float, axis=-1, keepdims=True) + 1e-06)
        * moe_gain.astype(jnp.float32)
    ).astype(jnp.bfloat16)
    flat_ids = routes.reshape(-1)
    onehot = (flat_ids[:, None] == jnp.arange(experts, dtype=jnp.int32)[None, :]).astype(jnp.int32)
    slot_rank = jnp.sum((jnp.cumsum(onehot, axis=0) - onehot) * onehot, axis=1)
    target = flat_ids * capacity + slot_rank
    source_row = (
        jnp.zeros((experts * capacity,), jnp.int32)
        .at[target]
        .set(jnp.arange(2 * row_count, dtype=jnp.int32) // 2)
    )
    outgoing = normed[source_row].reshape(experts, capacity, feat_width)
    w_gate = gate_proj[0]
    w_up = up_proj[0]
    w_down = down_proj[0]
    share_size = capacity // lax.axis_size(TP)
    own_share = lax.dynamic_slice_in_dim(outgoing, lax.axis_index(TP) * share_size, share_size, 1)
    arrived_share = lax.all_to_all(own_share, EP, split_axis=0, concat_axis=0, tiled=True)
    arrived = collect(arrived_share, TP, 1)
    gate_part = jnp.einsum("scd,df->scf", arrived, w_gate, preferred_element_type=jnp.float32)
    up_part = jnp.einsum("scd,df->scf", arrived, w_up, preferred_element_type=jnp.float32)
    hidden = (jax.nn.silu(gate_part) * up_part).astype(jnp.bfloat16)
    expert_out = jnp.einsum(
        "scf,fd->scd",
        lax.all_gather(hidden, TP, axis=2, tiled=True),
        w_down,
        preferred_element_type=jnp.float32,
    ).astype(jnp.bfloat16)
    returned = lax.all_to_all(expert_out, EP, split_axis=0, concat_axis=0, tiled=True)
    picked = returned.reshape(experts * capacity, -1)[target].reshape(row_count, 2, -1)
    return jnp.sum(picked.astype(jnp.float32) * route_weights[:, :, None], axis=1).astype(
        jnp.bfloat16
    )


def on_device(
    queries,
    keys,
    values,
    gates,
    log_decay,
    out_weight,
    moe_rows,
    moe_gain,
    routes,
    route_weights,
    gate_proj,
    up_proj,
    down_proj,
):
    mixer_out = retention_half(queries, keys, values, gates, log_decay, out_weight)
    moe_out = expert_half(moe_rows, moe_gain, routes, route_weights, gate_proj, up_proj, down_proj)
    return (mixer_out, moe_out)


def solution(mesh):
    torus = Mesh(mesh.devices.reshape(16, 2, 4, 4), ("ep_0", "ep_1", "tp_0", "tp_1"))
    return jax.shard_map(
        on_device,
        mesh=torus,
        in_specs=(
            P(EP, TP),
            P(EP, TP),
            P(EP, TP),
            P(EP, TP),
            P(EP, TP),
            P(None, TP),
            P(EP, None),
            P(),
            P(EP, None),
            P(EP, None),
            P(EP, None, TP),
            P(EP, None, TP),
            P(EP, None, TP),
        ),
        out_specs=(P(EP, TP), P(EP, TP)),
        check_vma=False,
    )
```

profile of v0, /device:TPU:2, one launch (start us, length us, event | category | flops | bytes accessed | tf_op | source)
XLA Modules:
  0.0 250.1 jit_solution(12538296000440214369)
XLA Ops:
  7.2 1.0 copy.44
  8.4 0.7 broadcast_multiply_fusion
  9.1 1.2 reduce-window.18
  11.0 2.4 scatter_custom_fusion
  13.5 0.7 convert_element_type.89
  14.2 1.5 fusion
  16.0 3.3 %gather_fusion = bf16[512,2048]{1,0:T(8,128)(2,1)} fusion(bf16[256,2048]{1,0:T(8,128)(2,1)S(1)} %fusion.2, s32[1024]{0:T(1024)S(1)} %pad_clamp_fusion.1), kind=kCustom, calls=%fused_computation | custom fusion | bytes 4196352 | tf_op jit(solution)/shard_map/gather | solution.py:173
  19.4 1.5 constant_dynamic-slice_fusion.1
  20.9 0.5 broadcast.370
  21.4 1.4 reduce.10
  22.8 0.7 reshape.656
  23.5 15.5 %all-to-all-start = ((bf16[32,2,1024]{2,1,0:T(2,128)(2,1)}), bf16[32,2,1024]{2,1,0:T(2,128)(2,1)S(1)}, u32[]{:S(2)}, u32[]{:S(2)}) async-start(bf16[32,2,1024]{2,1,0:T(2,128)(2,1)} %reshape.656), calls=%async_computation | async-start | bytes 262144 | tf_op jit(solution)/shard_map/all_to_all | solution.py:179
  39.4 0.6 slice_reduce_fusion.1
  40.2 0.6 fusion.34
  40.9 0.6 fusion.80
  41.9 2.4 while.13
  41.9 0.6 fusion.88
  42.5 0.6 bitcast_add_fusion.2
  43.1 0.6 fusion.88
  43.7 0.6 bitcast_add_fusion.2
  44.9 0.5 pad_bitcast_fusion.1
  45.5 10.7 %all-to-all-done = bf16[32,2,1024]{2,1,0:T(2,128)(2,1)S(1)} async-done(((bf16[32,2,1024]{2,1,0:T(2,128)(2,1)}), bf16[32,2,1024]{2,1,0:T(2,128)(2,1)S(1)}, u32[]{:S(2)}, u32[]{:S(2)}) %all-to-all-start) | async-done | bytes 131104 | tf_op jit(solution)/shard_map/all_to_all | solution.py:179
  56.4 1.6 broadcast_in_dim.33
  58.0 7.5 %all-to-all-start.1 = ((bf16[16,32,1,2048]{3,1,2,0:T(8,128)(2,1)}), bf16[16,32,1,2048]{3,1,2,0:T(8,128)(2,1)S(1)}, u32[]{:S(2)}, u32[]{:S(2)}) async-start(bf16[16,32,1,2048]{3,1,2,0:T(8,128)(2,1)} %broadcast_in_dim.33), calls=%async_computation.1 | async-start | bytes 4194304 | tf_op jit(solution)/shard_map/all_to_all | solution.py:64
  65.6 1.9 all-gather.2
  67.5 0.6 fusion.79
  70.0 0.7 fusion.66
  70.6 0.6 maximum_bitcast_fusion.1
  71.3 20.4 %all-to-all-done.1 = bf16[16,32,1,2048]{3,1,2,0:T(8,128)(2,1)S(1)} async-done(((bf16[16,32,1,2048]{3,1,2,0:T(8,128)(2,1)}), bf16[16,32,1,2048]{3,1,2,0:T(8,128)(2,1)S(1)}, u32[]{:S(2)}, u32[]{:S(2)}) %all-to-all-start.1) | async-done | bytes 2097184 | tf_op jit(solution)/shard_map/all_to_all | solution.py:64
  91.7 0.7 fusion.5
  92.5 0.5 copy-done.12
  92.9 1.4 fusion.10
  94.5 0.9 reduce-window.14
  96.0 0.6 fusion.72
  96.6 36.7 %all-gather.12.cloned.1.call-done = f32[16,129,128]{2,1,0:T(8,128)} async-done(((f32[1,129,128]{2,1,0:T(8,128)}), f32[16,129,128]{2,1,0:T(8,128)}) %all-gather.12.cloned.1.call-update) | async-done | bytes 1056784 | tf_op jit(solution)/shard_map/all_gather | solution.py:26
  133.3 0.8 slice.250
  134.2 0.6 fusion.78
  135.4 11.5 %fusion.57 = f32[128,128]{1,0:T(8,128)S(1)} fusion(f32[16,129,128]{2,1,0:T(8,128)} %all-gather.12.cloned.1.call-done, f32[2,129,128]{2,1,0:T(8,128)S(1)} %all-gather.2, f32[]{:T(128)} %bitcast.46, f32[]{:T(128)} %bitcast.45, f32[]{:T(128)} %bitcast.44, f32[]{:T(128)} %bitcast.43, f32[]{:T(128)} %bitcast.42, f32[]{:T(128)} %bitcast.41, f32[]{:T(128)} %bitcast.40, ...), kind=kLoop, calls=%fused_computation.81 | loop fusion | flops 884736 | bytes 1245278 | tf_op jit(solution)/shard_map/mul | solution.py:136
  146.9 1.2 fusion.14
  148.7 13.4 %all_gather.25 = bf16[256,512]{1,0:T(8,128)(2,1)} all-gather(bf16[256,128]{1,0:T(8,128)(2,1)S(1)} %fusion.50), channel_id=1, replica_groups=mesh['ep_0'=16,'ep_1'=2,'tp_0'=4,'tp_1'=4] {'tp_1'}, dimensions={1}, use_global_device_ids=true | all-gather | bytes 327680 | tf_op jit(solution)/shard_map/all_gather | solution.py:52
  162.2 43.0 %all-gather.10.cloned.1.call-done = bf16[32,16,4096]{2,0,1:T(8,128)(2,1)} async-done(((bf16[32,16,256]{2,0,1:T(8,128)(2,1)}), bf16[32,16,4096]{2,0,1:T(8,128)(2,1)}) %all-gather.10.cloned.1.call-update) | async-done | bytes 4194320 | tf_op jit(solution)/shard_map/all_gather | solution.py:186
  205.2 3.4 %fusion.16 = bf16[32,16,128]{2,0,1:T(8,128)(2,1)S(1)} fusion(bf16[32,16,4096]{2,0,1:T(8,128)(2,1)} %all-gather.10.cloned.1.call-done, bf16[1,4096,128]{2,1,0:T(8,128)(2,1)S(1)} %copy-done.13), kind=kOutput, calls=%fused_computation.25 | convolution fusion | flops 536870912 | bytes 5373952 | tf_op jit(solution)/shard_map/scf,fd->scd/dot_general | solution.py:184
  208.6 0.7 copy.58
  209.3 12.6 %all-to-all-start.2 = ((bf16[32,16,128]{2,1,0:T(8,128)(2,1)}), bf16[32,16,128]{2,1,0:T(8,128)(2,1)S(1)}, u32[]{:S(2)}, u32[]{:S(2)}) async-start(bf16[32,16,128]{2,1,0:T(8,128)(2,1)} %copy.58), calls=%async_computation.2 | async-start | bytes 262144 | tf_op jit(solution)/shard_map/all_to_all | solution.py:190
  222.1 16.8 %all-gather.8.cloned.1.call-done = bf16[256,2048]{1,0:T(8,128)(2,1)} async-done(((bf16[256,512]{1,0:T(8,128)(2,1)}), bf16[256,2048]{1,0:T(8,128)(2,1)}) %all-gather.8.cloned.1.call-update) | async-done | bytes 1048592 | tf_op jit(solution)/shard_map/all_gather | solution.py:52
  238.9 2.3 convolution_convert_fusion
  241.2 1.3 gather_fusion.1
  242.5 1.1 fusion.20
  (72 shorter events, 3.4 us)
Async XLA Ops:
  7.2 84.6 %copy-start = (bf16[1,2048,256]{2,1,0:T(8,128)(2,1)S(1)}, bf16[1,2048,256]{2,1,0:T(8,128)(2,1)}, u32[]{:S(2)}) copy-start(bf16[1,2048,256]{2,1,0:T(8,128)(2,1)} %param.25) | copy-start | bytes 3145732
  7.2 8.5 %copy-start.1 = (bf16[256,2048]{1,0:T(8,128)(2,1)S(1)}, bf16[256,2048]{1,0:T(8,128)(2,1)}, u32[]{:S(2)}) copy-start(bf16[256,2048]{1,0:T(8,128)(2,1)} %param.21) | copy-start | bytes 3145732
  16.0 23.1 %copy-start.10 = (f32[256,1]{0,1:T(1,128)S(1)}, f32[256,1]{0,1:T(1,128)}, u32[]{:S(2)}) copy-start(f32[256,1]{0,1:T(1,128)} %param.19) | copy-start | bytes 3076
  16.0 24.1 %copy-start.4 = (bf16[256,128]{1,0:T(8,128)(2,1)S(1)}, bf16[256,128]{1,0:T(8,128)(2,1)}, u32[]{:S(2)}) copy-start(bf16[256,128]{1,0:T(8,128)(2,1)} %param.16) | copy-start | bytes 196612
  16.0 24.1 %copy-start.5 = (bf16[256,128]{1,0:T(8,128)(2,1)S(1)}, bf16[256,128]{1,0:T(8,128)(2,1)}, u32[]{:S(2)}) copy-start(bf16[256,128]{1,0:T(8,128)(2,1)} %param.15) | copy-start | bytes 196612
  19.4 22.1 %copy-start.6 = (bf16[256,128]{1,0:T(8,128)(2,1)S(1)}, bf16[256,128]{1,0:T(8,128)(2,1)}, u32[]{:S(2)}) copy-start(bf16[256,128]{1,0:T(8,128)(2,1)} %param.17) | copy-start | bytes 196612
  23.5 32.7 %all-to-all-start = ((bf16[32,2,1024]{2,1,0:T(2,128)(2,1)}), bf16[32,2,1024]{2,1,0:T(2,128)(2,1)S(1)}, u32[]{:S(2)}, u32[]{:S(2)}) async-start(bf16[32,2,1024]{2,1,0:T(2,128)(2,1)} %reshape.656), calls=%async_computation | async-start | bytes 262144 | tf_op jit(solution)/shard_map/all_to_all | solution.py:179
  44.3 1.2 copy-start.3
  44.3 13.7 %copy-start.9 = (f32[2,1]{0,1:T(1,128)}, f32[2,1]{0,1:T(1,128)S(1)}, u32[]{:S(2)}) copy-start(f32[2,1]{0,1:T(1,128)S(1)} %get-tuple-element.178) | copy-start | bytes 28
  58.0 7.5 %copy-start.11 = (f32[1,128]{1,0:T(1,128)S(1)}, f32[1,128]{1,0:T(1,128)}, u32[]{:S(2)}) copy-start(f32[1,128]{1,0:T(1,128)} %pad_bitcast_fusion.1) | copy-start | bytes 1540
  58.0 33.7 %all-to-all-start.1 = ((bf16[16,32,1,2048]{3,1,2,0:T(8,128)(2,1)}), bf16[16,32,1,2048]{3,1,2,0:T(8,128)(2,1)S(1)}, u32[]{:S(2)}, u32[]{:S(2)}) async-start(bf16[16,32,1,2048]{3,1,2,0:T(8,128)(2,1)} %broadcast_in_dim.33), calls=%async_computation.1 | async-start | bytes 4194304 | tf_op jit(solution)/shard_map/all_to_all | solution.py:64
  65.5 67.8 %all-gather.12.cloned.1.call-start = ((), (), s32[]{:S(2)}) async-start(), calls=%async_computation.5 | async-start | bytes 1183744 | tf_op jit(solution)/shard_map/all_gather | solution.py:26
  71.3 133.9 %all-gather.10.cloned.1.call-start = ((), (), s32[]{:S(2)}) async-start(), calls=%async_computation.4 | async-start | bytes 4456448 | tf_op jit(solution)/shard_map/all_gather | solution.py:186
  91.7 1.2 copy-start.12
  94.4 54.2 %copy-start.7 = (bf16[256,128]{1,0:T(8,128)(2,1)S(1)}, bf16[256,128]{1,0:T(8,128)(2,1)}, u32[]{:S(2)}) copy-start(bf16[256,128]{1,0:T(8,128)(2,1)} %param.18) | copy-start | bytes 196612
  94.4 110.8 %copy-start.13 = (bf16[1,4096,128]{2,1,0:T(8,128)(2,1)S(1)}, bf16[1,4096,128]{2,1,0:T(8,128)(2,1)}, u32[]{:S(2)}) copy-start(bf16[1,4096,128]{2,1,0:T(8,128)(2,1)} %param.27) | copy-start | bytes 3145732
  94.4 144.5 %all-gather.8.cloned.1.call-start = ((), (), s32[]{:S(2)}) async-start(), calls=%async_computation.3 | async-start | bytes 1310720 | tf_op jit(solution)/shard_map/all_gather | solution.py:52
  162.1 59.7 %copy-start.8 = (f32[256,2]{0,1:T(2,128)S(1)}, f32[256,2]{0,1:T(2,128)}, u32[]{:S(2)}) copy-start(f32[256,2]{0,1:T(2,128)} %param.24) | copy-start | bytes 6148
  162.2 76.7 %copy-start.2 = (bf16[2048,128]{1,0:T(8,128)(2,1)S(1)}, bf16[2048,128]{1,0:T(8,128)(2,1)}, u32[]{:S(2)}) copy-start(bf16[2048,128]{1,0:T(8,128)(2,1)} %param.20) | copy-start | bytes 1572868
  209.3 31.9 %all-to-all-start.2 = ((bf16[32,16,128]{2,1,0:T(8,128)(2,1)}), bf16[32,16,128]{2,1,0:T(8,128)(2,1)S(1)}, u32[]{:S(2)}, u32[]{:S(2)}) async-start(bf16[32,16,128]{2,1,0:T(8,128)(2,1)} %copy.58), calls=%async_computation.2 | async-start | bytes 262144 | tf_op jit(solution)/shard_map/all_to_all | solution.py:190
Sparse Core Ops, SparseCore 0:
  71.4 61.8 all-gather.11
  136.3 68.8 all-gather.9
  207.3 31.5 all-gather.7
where the time goes:
time: 251 us; the launch traced here: 250 us
  waiting for transfers between devices  128 us (51%)
  starting transfers between devices  35.6 us (14%)
  other arithmetic  24.8 us (10%)
  local copies, waits for them, and re-layouts  18.7 us (7%)
  between operations  18 us (7%)
  blocking collectives  15.3 us (6%)
  matrix products  9.84 us (4%)
    all_gather x1, waiting for transfers between devices, expert_half(): lax.all_gather(hidden, TP, axis=2, tiled=True)  43 us
    all_gather x1, waiting for transfers between devices, collected_together(): both, at, found = (lax.all_gather(jnp.concatenate(lines), axis), 0, {})  36.7 us
    all_to_all x1, waiting for transfers between devices, copy_for_each(): lax.all_to_all(jnp.broadcast_to(array[None], (peers, *array.shape)), axis...  20.4 us
    all_gather x1, waiting for transfers between devices, whole_of(): array = lax.all_gather(array, axis, axis=dim, tiled=True)  16.8 us
    all_to_all x1, starting transfers between devices, expert_half(): lax.all_to_all(own_share, EP, split_axis=0, concat_axis=0, tiled=True)  15.5 us
    all_gather x1, blocking collectives, whole_of(): array = lax.all_gather(array, axis, axis=dim, tiled=True)  13.4 us
    all_to_all x1, starting transfers between devices, expert_half(): lax.all_to_all(expert_out, EP, split_axis=0, concat_axis=0, tiled=True)  12.6 us
    mul x1, other arithmetic, retention_half(): entering = before + jnp.exp(leading)[:, :, None, None] * incoming[1][None]  11.5 us
  transfers between devices with their start and end apart: 6, of which 5 were waited for; matrix products, arithmetic and copies ran while one was open for 13% of the time, Pallas kernels for 0%

commit v1 on v0

--- a/solution.py
+++ b/solution.py
@@ -7,6 +7,12 @@
 BLOCK = 128
 EP = ("ep_0", "ep_1")
 TP = ("tp_0", "tp_1")
+
+
+def gather_blocks(shard, axis, dim):
+    pieces = lax.all_gather(shard, axis, axis=0, tiled=False)
+    whole = jnp.concatenate(pieces, axis=dim)
+    return whole
 
 
 def filled_with(array, identity):
@@ -182,10 +188,7 @@
     up_part = jnp.einsum("scd,df->scf", arrived, w_up, preferred_element_type=jnp.float32)
     hidden = (jax.nn.silu(gate_part) * up_part).astype(jnp.bfloat16)
     expert_out = jnp.einsum(
-        "scf,fd->scd",
-        lax.all_gather(hidden, TP, axis=2, tiled=True),
-        w_down,
-        preferred_element_type=jnp.float32,
+        "scf,fd->scd", gather_blocks(hidden, TP, 2), w_down, preferred_element_type=jnp.float32
     ).astype(jnp.bfloat16)
     returned = lax.all_to_all(expert_out, EP, split_axis=0, concat_axis=0, tiled=True)
     picked = returned.reshape(experts * capacity, -1)[target].reshape(row_count, 2, -1)

time: 251 us -> 260 us (1.036)
  local copies, waits for them, and re-layouts: 18.7 us -> 33.9 us
  waiting for transfers between devices: 128 us -> 123 us
    all_gather x1, waiting for transfers between devices: 16.8 us -> 1.73 us  [whole_of(): array = lax.all_gather(array, axis, axis=dim, tiled=True)]
    all_to_all x1, waiting for transfers between devices: 0.01 us -> 13 us  [expert_half(): lax.all_to_all(expert_out, EP, split_axis=0, concat_axis=0, tiled=True)]
    all_gather x0 -> x1, local copies, waits for them, and re-layouts: none -> 7.58 us  [gather_blocks(): pieces = lax.all_gather(shard, axis, axis=0, tiled=False)]
    reshape x0 -> x1, local copies, waits for them, and re-layouts: none -> 7.5 us  [gather_blocks(): whole = jnp.concatenate(pieces, axis=dim)]
    all_gather x1, waiting for transfers between devices: 43 us -> 40.4 us  [gather_blocks(): pieces = lax.all_gather(shard, axis, axis=0, tiled=False)]
  transfers between devices with their start and end apart: 6 -> 6, of which waited for: 5 -> 6; matrix products, arithmetic and copies ran while one was open for 13% -> 18% of each run, Pallas kernels for 0% -> 0%
where the time goes in v1:
time: 260 us; the launch traced here: 259 us
  waiting for transfers between devices  123 us (47%)
  starting transfers between devices  35.7 us (14%)
  local copies, waits for them, and re-layouts  33.9 us (13%)
  other arithmetic  24.7 us (10%)
  between operations  18.1 us (7%)
  blocking collectives  14.6 us (6%)
  matrix products  8.96 us (3%)
    all_gather x1, waiting for transfers between devices, gather_blocks(): pieces = lax.all_gather(shard, axis, axis=0, tiled=False)  40.4 us
    all_gather x1, waiting for transfers between devices, collected_together(): both, at, found = (lax.all_gather(jnp.concatenate(lines), axis), 0, {})  36.6 us
    all_to_all x1, waiting for transfers between devices, copy_for_each(): lax.all_to_all(jnp.broadcast_to(array[None], (peers, *array.shape)), axis...  20.4 us
    all_to_all x1, starting transfers between devices, expert_half(): lax.all_to_all(own_share, EP, split_axis=0, concat_axis=0, tiled=True)  15.5 us
    all_to_all x1, waiting for transfers between devices, expert_half(): lax.all_to_all(expert_out, EP, split_axis=0, concat_axis=0, tiled=True)  13 us
    all_gather x1, blocking collectives, whole_of(): array = lax.all_gather(array, axis, axis=dim, tiled=True)  12.7 us
    all_to_all x1, starting transfers between devices, expert_half(): lax.all_to_all(expert_out, EP, split_axis=0, concat_axis=0, tiled=True)  12.6 us
    mul x1, other arithmetic, retention_half(): entering = before + jnp.exp(leading)[:, :, None, None] * incoming[1][None]  11.5 us
  transfers between devices with their start and end apart: 6, of which 6 were waited for; matrix products, arithmetic and copies ran while one was open for 18% of the time, Pallas kernels for 0%

profile of v1, /device:TPU:2, one launch (start us, length us, event | category | flops | bytes accessed | tf_op | source)
XLA Modules:
  0.0 258.8 jit_solution(13104135569204509674)
XLA Ops:
  7.2 1.0 copy.47
  8.4 0.7 broadcast_multiply_fusion
  9.1 1.2 reduce-window.18
  11.0 2.4 scatter_custom_fusion
  13.5 0.7 convert_element_type.89
  14.2 1.5 fusion
  16.0 3.3 %gather_fusion = bf16[512,2048]{1,0:T(8,128)(2,1)} fusion(bf16[256,2048]{1,0:T(8,128)(2,1)S(1)} %fusion.2, s32[1024]{0:T(1024)S(1)} %pad_clamp_fusion.1), kind=kCustom, calls=%fused_computation | custom fusion | bytes 4196352 | tf_op jit(solution)/shard_map/gather | solution.py:179
  19.4 1.5 constant_dynamic-slice_fusion.1
  21.4 1.4 reduce.10
  22.8 0.7 reshape.665
  23.5 15.5 %all-to-all-start = ((bf16[32,2,1024]{2,1,0:T(2,128)(2,1)}), bf16[32,2,1024]{2,1,0:T(2,128)(2,1)S(1)}, u32[]{:S(2)}, u32[]{:S(2)}) async-start(bf16[32,2,1024]{2,1,0:T(2,128)(2,1)} %reshape.665), calls=%async_computation | async-start | bytes 262144 | tf_op jit(solution)/shard_map/all_to_all | solution.py:185
  39.4 0.6 slice_reduce_fusion.1
  40.2 0.6 fusion.33
  40.9 0.6 fusion.79
  41.9 2.4 while.13
  41.9 0.6 fusion.87
  42.5 0.6 bitcast_add_fusion.2
  43.1 0.6 fusion.87
  43.7 0.6 bitcast_add_fusion.2
  44.9 0.5 pad_bitcast_fusion.1
  45.5 10.7 %all-to-all-done = bf16[32,2,1024]{2,1,0:T(2,128)(2,1)S(1)} async-done(((bf16[32,2,1024]{2,1,0:T(2,128)(2,1)}), bf16[32,2,1024]{2,1,0:T(2,128)(2,1)S(1)}, u32[]{:S(2)}, u32[]{:S(2)}) %all-to-all-start) | async-done | bytes 131104 | tf_op jit(solution)/shard_map/all_to_all | solution.py:185
  56.4 1.6 broadcast_in_dim.33
  58.0 7.5 %all-to-all-start.1 = ((bf16[16,32,1,2048]{3,1,2,0:T(8,128)(2,1)}), bf16[16,32,1,2048]{3,1,2,0:T(8,128)(2,1)S(1)}, u32[]{:S(2)}, u32[]{:S(2)}) async-start(bf16[16,32,1,2048]{3,1,2,0:T(8,128)(2,1)} %broadcast_in_dim.33), calls=%async_computation.1 | async-start | bytes 4194304 | tf_op jit(solution)/shard_map/all_to_all | solution.py:70
  65.6 1.9 all-gather.3
  67.5 0.6 fusion.78
  70.0 0.7 fusion.65
  70.6 0.6 maximum_bitcast_fusion.1
  71.3 20.4 %all-to-all-done.1 = bf16[16,32,1,2048]{3,1,2,0:T(8,128)(2,1)S(1)} async-done(((bf16[16,32,1,2048]{3,1,2,0:T(8,128)(2,1)}), bf16[16,32,1,2048]{3,1,2,0:T(8,128)(2,1)S(1)}, u32[]{:S(2)}, u32[]{:S(2)}) %all-to-all-start.1) | async-done | bytes 2097184 | tf_op jit(solution)/shard_map/all_to_all | solution.py:70
  91.7 0.7 fusion.5
  92.9 0.7 fusion.10
  93.7 0.8 copy.51
  94.6 0.8 reduce-window.14
  96.1 0.6 fusion.71
  96.7 36.6 %all-gather.13.cloned.1.call-done = f32[16,129,128]{2,1,0:T(8,128)} async-done(((f32[1,129,128]{2,1,0:T(8,128)}), f32[16,129,128]{2,1,0:T(8,128)}) %all-gather.13.cloned.1.call-update) | async-done | bytes 1056784 | tf_op jit(solution)/shard_map/all_gather | solution.py:32
  133.3 0.8 slice.250
  134.1 0.6 fusion.77
  135.4 11.5 %fusion.56 = f32[128,128]{1,0:T(8,128)S(1)} fusion(f32[16,129,128]{2,1,0:T(8,128)} %all-gather.13.cloned.1.call-done, f32[2,129,128]{2,1,0:T(8,128)S(1)} %all-gather.3, f32[]{:T(128)} %bitcast.46, f32[]{:T(128)} %bitcast.45, f32[]{:T(128)} %bitcast.44, f32[]{:T(128)} %bitcast.43, f32[]{:T(128)} %bitcast.42, f32[]{:T(128)} %bitcast.41, f32[]{:T(128)} %bitcast.40, ...), kind=kLoop, calls=%fused_computation.81 | loop fusion | flops 884736 | bytes 1245278 | tf_op jit(solution)/shard_map/mul | solution.py:142
  147.8 12.7 %all_gather.28 = bf16[256,512]{1,0:T(8,128)(2,1)} all-gather(bf16[256,128]{1,0:T(8,128)(2,1)S(1)} %fusion.49), channel_id=1, replica_groups=mesh['ep_0'=16,'ep_1'=2,'tp_0'=4,'tp_1'=4] {'tp_1'}, dimensions={1}, use_global_device_ids=true | all-gather | bytes 327680 | tf_op jit(solution)/shard_map/all_gather | solution.py:58
  160.5 40.4 %all-gather.11.cloned.1.call-done = bf16[512,16,256]{2,1,0:T(8,128)(2,1)} async-done(((bf16[32,16,256]{2,1,0:T(8,128)(2,1)}), bf16[512,16,256]{2,1,0:T(8,128)(2,1)}) %all-gather.11.cloned.1.call-update) | async-done | bytes 4194320 | tf_op jit(solution)/shard_map/all_gather | solution.py:13
  200.9 7.6 %copy.60 = bf16[16,32,16,256]{3,0,2,1:T(8,128)(2,1)} copy(bf16[16,32,16,256]{3,2,1,0:T(8,128)(2,1)} %bitcast.165) | data formatting | bytes 8388608 | tf_op jit(solution)/shard_map/all_gather | solution.py:13
  208.4 7.5 %reshape.615 = bf16[32,16,4096]{2,1,0:T(8,128)(2,1)} reshape(bf16[32,16,16,256]{3,2,1,0:T(8,128)(2,1)} %bitcast.162) | data formatting | bytes 8388608 | tf_op jit(solution)/shard_map/reshape | solution.py:14
  215.9 4.1 %convolution_convert_fusion = bf16[32,16,128]{2,1,0:T(8,128)(2,1)} fusion(bf16[32,16,4096]{2,1,0:T(8,128)(2,1)} %reshape.615, bf16[1,4096,128]{2,1,0:T(8,128)(2,1)S(1)} %copy-done.15), kind=kOutput, calls=%fused_computation.18 | convolution fusion | flops 536936448 | bytes 5373952 | tf_op jit(solution)/shard_map/scf,fd->scd/dot_general | solution.py:190
  220.1 12.6 %all-to-all-start.2 = ((bf16[32,16,128]{2,1,0:T(8,128)(2,1)}), bf16[32,16,128]{2,1,0:T(8,128)(2,1)S(1)}, u32[]{:S(2)}, u32[]{:S(2)}) async-start(bf16[32,16,128]{2,1,0:T(8,128)(2,1)} %convolution_convert_fusion), calls=%async_computation.2 | async-start | bytes 262144 | tf_op jit(solution)/shard_map/all_to_all | solution.py:193
  232.8 1.7 all-gather.9.cloned.1.call-done
  234.6 2.3 convolution_convert_fusion.1
  236.9 13.0 %all-to-all-done.2 = bf16[32,16,128]{2,1,0:T(8,128)(2,1)S(1)} async-done(((bf16[32,16,128]{2,1,0:T(8,128)(2,1)}), bf16[32,16,128]{2,1,0:T(8,128)(2,1)S(1)}, u32[]{:S(2)}, u32[]{:S(2)}) %all-to-all-start.2) | async-done | bytes 131104 | tf_op jit(solution)/shard_map/all_to_all | solution.py:193
  249.9 1.3 gather_fusion.1
  251.2 1.1 fusion.19
  (78 shorter events, 4.7 us)
Async XLA Ops:
  7.2 84.6 %copy-start = (bf16[1,2048,256]{2,1,0:T(8,128)(2,1)S(1)}, bf16[1,2048,256]{2,1,0:T(8,128)(2,1)}, u32[]{:S(2)}) copy-start(bf16[1,2048,256]{2,1,0:T(8,128)(2,1)} %param.25) | copy-start | bytes 3145732
  7.2 8.5 %copy-start.1 = (bf16[256,2048]{1,0:T(8,128)(2,1)S(1)}, bf16[256,2048]{1,0:T(8,128)(2,1)}, u32[]{:S(2)}) copy-start(bf16[256,2048]{1,0:T(8,128)(2,1)} %param.21) | copy-start | bytes 3145732
  16.0 23.1 %copy-start.12 = (f32[256,1]{0,1:T(1,128)S(1)}, f32[256,1]{0,1:T(1,128)}, u32[]{:S(2)}) copy-start(f32[256,1]{0,1:T(1,128)} %param.19) | copy-start | bytes 3076
  16.0 24.1 %copy-start.5 = (bf16[256,128]{1,0:T(8,128)(2,1)S(1)}, bf16[256,128]{1,0:T(8,128)(2,1)}, u32[]{:S(2)}) copy-start(bf16[256,128]{1,0:T(8,128)(2,1)} %param.16) | copy-start | bytes 196612
  16.0 24.1 %copy-start.6 = (bf16[256,128]{1,0:T(8,128)(2,1)S(1)}, bf16[256,128]{1,0:T(8,128)(2,1)}, u32[]{:S(2)}) copy-start(bf16[256,128]{1,0:T(8,128)(2,1)} %param.15) | copy-start | bytes 196612
  19.4 22.1 %copy-start.7 = (bf16[256,128]{1,0:T(8,128)(2,1)S(1)}, bf16[256,128]{1,0:T(8,128)(2,1)}, u32[]{:S(2)}) copy-start(bf16[256,128]{1,0:T(8,128)(2,1)} %param.17) | copy-start | bytes 196612
  23.5 32.7 %all-to-all-start = ((bf16[32,2,1024]{2,1,0:T(2,128)(2,1)}), bf16[32,2,1024]{2,1,0:T(2,128)(2,1)S(1)}, u32[]{:S(2)}, u32[]{:S(2)}) async-start(bf16[32,2,1024]{2,1,0:T(2,128)(2,1)} %reshape.665), calls=%async_computation | async-start | bytes 262144 | tf_op jit(solution)/shard_map/all_to_all | solution.py:185
  44.3 13.8 %copy-start.3 = (f32[2,1,128,128]{3,2,1,0:T(8,128)}, f32[2,1,128,128]{3,2,1,0:T(8,128)S(1)}, u32[]{:S(2)}) copy-start(f32[2,1,128,128]{3,2,1,0:T(8,128)S(1)} %get-tuple-element.30) | copy-start | bytes 393220
  44.3 13.7 %copy-start.11 = (f32[2,1]{0,1:T(1,128)}, f32[2,1]{0,1:T(1,128)S(1)}, u32[]{:S(2)}) copy-start(f32[2,1]{0,1:T(1,128)S(1)} %get-tuple-element.179) | copy-start | bytes 28
  58.0 7.5 %copy-start.13 = (f32[1,128]{1,0:T(1,128)S(1)}, f32[1,128]{1,0:T(1,128)}, u32[]{:S(2)}) copy-start(f32[1,128]{1,0:T(1,128)} %pad_bitcast_fusion.1) | copy-start | bytes 1540
  58.0 33.7 %all-to-all-start.1 = ((bf16[16,32,1,2048]{3,1,2,0:T(8,128)(2,1)}), bf16[16,32,1,2048]{3,1,2,0:T(8,128)(2,1)S(1)}, u32[]{:S(2)}, u32[]{:S(2)}) async-start(bf16[16,32,1,2048]{3,1,2,0:T(8,128)(2,1)} %broadcast_in_dim.33), calls=%async_computation.1 | async-start | bytes 4194304 | tf_op jit(solution)/shard_map/all_to_all | solution.py:70
  65.5 67.8 %all-gather.13.cloned.1.call-start = ((), (), s32[]{:S(2)}) async-start(), calls=%async_computation.5 | async-start | bytes 1183744 | tf_op jit(solution)/shard_map/all_gather | solution.py:32
  71.3 129.6 %all-gather.11.cloned.1.call-start = ((), (), s32[]{:S(2)}) async-start(), calls=%async_computation.4 | async-start | bytes 4456448 | tf_op jit(solution)/shard_map/all_gather | solution.py:13
  91.7 1.2 copy-start.14
  93.7 53.2 %copy-start.4 = (f32[2,1,128,128]{3,2,1,0:T(8,128)S(1)}, f32[2,1,128,128]{3,2,1,0:T(8,128)}, u32[]{:S(2)}) copy-start(f32[2,1,128,128]{3,2,1,0:T(8,128)} %copy-done.3) | copy-start | bytes 393220
  93.7 53.2 %copy-start.9 = (f32[2,128]{1,0:T(2,128)S(1)}, f32[2,128]{1,0:T(2,128)}, u32[]{:S(2)}) copy-start(f32[2,128]{1,0:T(2,128)} %get-tuple-element.106) | copy-start | bytes 3076
  93.7 54.0 %copy-start.8 = (bf16[256,128]{1,0:T(8,128)(2,1)S(1)}, bf16[256,128]{1,0:T(8,128)(2,1)}, u32[]{:S(2)}) copy-start(bf16[256,128]{1,0:T(8,128)(2,1)} %param.18) | copy-start | bytes 196612
  94.6 140.0 %all-gather.9.cloned.1.call-start = ((), (), s32[]{:S(2)}) async-start(), calls=%async_computation.3 | async-start | bytes 1310720 | tf_op jit(solution)/shard_map/all_gather | solution.py:58
  208.4 7.5 %copy-start.15 = (bf16[1,4096,128]{2,1,0:T(8,128)(2,1)S(1)}, bf16[1,4096,128]{2,1,0:T(8,128)(2,1)}, u32[]{:S(2)}) copy-start(bf16[1,4096,128]{2,1,0:T(8,128)(2,1)} %param.27) | copy-start | bytes 3145732
  215.9 16.7 %copy-start.10 = (f32[256,2]{0,1:T(2,128)S(1)}, f32[256,2]{0,1:T(2,128)}, u32[]{:S(2)}) copy-start(f32[256,2]{0,1:T(2,128)} %param.24) | copy-start | bytes 6148
  215.9 18.6 %copy-start.2 = (bf16[2048,128]{1,0:T(8,128)(2,1)S(1)}, bf16[2048,128]{1,0:T(8,128)(2,1)}, u32[]{:S(2)}) copy-start(bf16[2048,128]{1,0:T(8,128)(2,1)} %param.20) | copy-start | bytes 1572868
  220.1 29.8 %all-to-all-start.2 = ((bf16[32,16,128]{2,1,0:T(8,128)(2,1)}), bf16[32,16,128]{2,1,0:T(8,128)(2,1)S(1)}, u32[]{:S(2)}, u32[]{:S(2)}) async-start(bf16[32,16,128]{2,1,0:T(8,128)(2,1)} %convolution_convert_fusion), calls=%async_computation.2 | async-start | bytes 262144 | tf_op jit(solution)/shard_map/all_to_all | solution.py:193
Sparse Core Ops, SparseCore 0:
  71.4 61.8 all-gather.12
  136.3 64.5 all-gather.10
  203.0 31.5 all-gather.8
